TPU v7x, 32 devices: a whole 2x2x4 slice. The times are simulated.
32 devices in a mesh: grp: 2 (over y), fs: 4 (over z), tp: 4 (over x, core).
Axes of the slice: x: 2, y: 2, z: 4, core: 2. Of those that a mesh axis runs over, the one named last changes fastest.
Arguments:
- tokens: bfloat16 [1024, 2048], P(('grp', 'fs')), parts along dimension 0, may hold values from -12 to 12, as said below
- mix_heads: bfloat16 [1024, 2048], P(('grp', 'fs'), 'tp'), parts along dimension 0, may hold values from -6 to 6
- norm_first: float32 [2048], replicated, may hold values from 0.1 to 1.9
- gate_first: bfloat16 [2048, 5632], P('fs', 'tp'), may hold values from -0.125 to 0.125
- up_first: bfloat16 [2048, 5632], P('fs', 'tp'), may hold values from -0.125 to 0.125
- down_first: bfloat16 [5632, 2048], P('tp', 'fs'), may hold values from -0.078125 to 0.078125
- out_weight: bfloat16 [2048, 2048], P('tp', 'fs'), may hold values from -0.125 to 0.125
- norm_second: float32 [2048], replicated, may hold values from 0.1 to 1.9
- gate_second: bfloat16 [2048, 5632], P('fs', 'tp'), may hold values from -0.125 to 0.125
- up_second: bfloat16 [2048, 5632], P('fs', 'tp'), may hold values from -0.125 to 0.125
- down_second: bfloat16 [5632, 2048], P('tp', 'fs'), may hold values from -0.078125 to 0.078125
Outputs:
- layer_out: bfloat16 [1024, 2048], P(('grp', 'fs')), parts along dimension 0
There are 2 independent parts, one for each index of `grp`. A program takes and returns all parts, laid end to end along the dimension named above; an argument that names none is the same for every part. Nothing has to cross between parts.
Inputs may be any that keep to these rules, and one draw needn't show every extreme that they name: Each row of tokens carries a scale of its own.
All inputs are finite; a program needn't handle non-finite values.
Results may differ from a plain program's by a relative error of at most 0.014.
Values may be sent and summed in bfloat16 or wider, within the bound.
A program may use at most 64 MiB of HBM per device.

v0:
```python
import jax
import jax.numpy as jnp
from jax import lax
from jax.sharding import PartitionSpec as P

EPS = 0.1


def norm_rows(row_block, gain_vector):
    widened = row_block.astype(jnp.float32)
    scaled = widened * lax.rsqrt(jnp.mean(widened * widened, axis=-1, keepdims=True) + EPS)
    return (scaled * gain_vector).astype(jnp.bfloat16)


def gate_values(normed, gate_weight, value_weight):
    whole_gate, whole_values = (
        lax.all_gather(gate_weight, "fs", axis=0, tiled=True),
        lax.all_gather(value_weight, "fs", axis=0, tiled=True),
    )
    return (
        jnp.dot(normed, whole_gate, preferred_element_type=jnp.float32),
        jnp.dot(normed, whole_values, preferred_element_type=jnp.float32),
    )


def half_branch(normed, gate_weight, value_weight, down_weight):
    gates, values = gate_values(normed, gate_weight, value_weight)
    hidden = (jax.nn.silu(gates) * values).astype(jnp.bfloat16)
    return 0.5 * jnp.dot(
        hidden,
        lax.all_gather(down_weight, "fs", axis=1, tiled=True),
        preferred_element_type=jnp.float32,
    )


def share_sum(block_terms):
    return lax.psum_scatter(
        block_terms.astype(jnp.bfloat16), "tp", scatter_dimension=0, tiled=True
    ).astype(jnp.float32)


def join_rows(row_block):
    return lax.all_gather(row_block, "tp", axis=0, tiled=True)


def local(
    tokens,
    mix_heads,
    norm_first,
    gate_first,
    up_first,
    down_first,
    out_weight,
    norm_second,
    gate_second,
    up_second,
    down_second,
):
    normed_one = norm_rows(tokens, norm_first)
    first_terms = half_branch(normed_one, gate_first, up_first, down_first)
    heads_out = jnp.dot(
        mix_heads,
        lax.all_gather(out_weight, "fs", axis=1, tiled=True),
        preferred_element_type=jnp.float32,
    )
    first_terms = first_terms + heads_out
    share_rows = tokens.shape[0] // lax.axis_size("tp")
    offset = lax.axis_index("tp") * share_rows
    own_rows = lax.dynamic_slice_in_dim(tokens, offset, share_rows, 0).astype(jnp.float32)
    resid_two = own_rows + share_sum(first_terms)
    normed_two = join_rows(norm_rows(resid_two, norm_second))
    second_terms = half_branch(normed_two, gate_second, up_second, down_second)
    finished = (resid_two + share_sum(second_terms)).astype(jnp.bfloat16)
    return join_rows(finished)


def solution(mesh):
    in_specs = (
        P(("grp", "fs"), None),
        P(("grp", "fs"), "tp"),
        P(),
        P("fs", "tp"),
        P("fs", "tp"),
        P("tp", "fs"),
        P("tp", "fs"),
        P(),
        P("fs", "tp"),
        P("fs", "tp"),
        P("tp", "fs"),
    )
    out_specs = P(("grp", "fs"), None)
    return jax.shard_map(local, mesh=mesh, in_specs=in_specs, out_specs=out_specs, check_vma=False)
```

profile of v0, /device:TPU:0, one launch (start us, length us, event | category | flops | bytes accessed | tf_op | source)
XLA Modules:
  0.0 763.6 jit_solution(13067139635178607233)
XLA Ops:
  6.5 0.0 copy-start
  6.5 0.0 all-gather.8.cloned.1.call-start
  6.5 0.7 all-gather.8.cloned.1.call-update
  7.3 0.0 copy-start.1
  7.3 0.0 copy-start.3
  7.3 0.0 all-gather.10.cloned.1.call-start
  7.3 0.7 all-gather.10.cloned.1.call-update
  8.0 0.0 all-gather.12.cloned.1.call-start
  8.1 0.7 all-gather.12.cloned.1.call-update
  8.8 0.0 all-gather.14.cloned.1.call-start
  8.8 0.5 all-gather.14.cloned.1.call-update
  9.3 0.0 reduce-scatter.3.cloned.1.call-start
  9.4 1.2 fusion.4
  10.6 107.7 %all-gather.8.cloned.1.call-done = bf16[2048,1408]{1,0:T(8,128)(2,1)} async-done(((bf16[512,1408]{1,0:T(8,128)(2,1)}), bf16[2048,1408]{1,0:T(8,128)(2,1)}) %all-gather.8.cloned.1.call-update) | async-done | bytes 5767184 | tf_op jit(solution)/shard_map/all_gather | solution.py:17
  118.3 3.9 fusion.11
  122.2 102.7 %all-gather.10.cloned.1.call-done = bf16[2048,1408]{1,0:T(8,128)(2,1)} async-done(((bf16[512,1408]{1,0:T(8,128)(2,1)}), bf16[2048,1408]{1,0:T(8,128)(2,1)}) %all-gather.10.cloned.1.call-update) | async-done | bytes 5767184 | tf_op jit(solution)/shard_map/all_gather | solution.py:18
  224.9 106.5 %all-gather.12.cloned.1.call-done = bf16[1408,2048]{1,0:T(8,128)(2,1)} async-done(((bf16[1408,512]{1,0:T(8,128)(2,1)}), bf16[1408,2048]{1,0:T(8,128)(2,1)}) %all-gather.12.cloned.1.call-update) | async-done | bytes 5767184 | tf_op jit(solution)/shard_map/all_gather | solution.py:31
  331.5 0.0 copy-done.1
  331.5 0.0 copy-done.3
  331.5 6.3 convolution_multiply_fusion.3
  337.8 0.0 copy-start.4
  337.8 39.1 %all-gather.14.cloned.1.call-done = bf16[512,2048]{1,0:T(8,128)(2,1)} async-done(((bf16[512,512]{1,0:T(8,128)(2,1)}), bf16[512,2048]{1,0:T(8,128)(2,1)}) %all-gather.14.cloned.1.call-update) | async-done | bytes 2097168 | tf_op jit(solution)/shard_map/all_gather | solution.py:63
  376.8 0.0 copy-done
  376.8 2.8 fusion
  379.7 0.0 reduce-scatter.3.cloned.1.call-update
  379.7 0.0 all-gather.16.cloned.1.call-start
  379.8 0.5 all-gather.16.cloned.1.call-update
  380.3 0.0 all-gather.18.cloned.1.call-start
  380.3 0.7 all-gather.18.cloned.1.call-update
  381.0 0.0 all-gather.20.cloned.1.call-start
  381.1 0.7 all-gather.20.cloned.1.call-update
  381.8 0.0 reduce-scatter.5.cloned.1.call-start
  381.8 18.5 %reduce-scatter.3.cloned.1.call-done = bf16[32,2048]{1,0:T(8,128)(2,1)} async-done(((bf16[128,2048]{1,0:T(8,128)(2,1)}), bf16[32,2048]{1,0:T(8,128)(2,1)}) %reduce-scatter.3.cloned.1.call-update) | async-done | bytes 131088 | tf_op jit(solution)/shard_map/reduce_scatter | solution.py:37
  400.3 1.1 multiply_reduce_fusion
  401.4 0.0 copy-done.4
  401.4 1.0 multiply_convert_fusion
  402.4 6.6 all_gather.31
  409.0 99.5 %all-gather.16.cloned.1.call-done = bf16[2048,1408]{1,0:T(8,128)(2,1)} async-done(((bf16[512,1408]{1,0:T(8,128)(2,1)}), bf16[2048,1408]{1,0:T(8,128)(2,1)}) %all-gather.16.cloned.1.call-update) | async-done | bytes 5767184 | tf_op jit(solution)/shard_map/all_gather | solution.py:17
  508.5 3.6 fusion.15
  512.1 0.0 copy-start.2
  512.1 102.9 %all-gather.18.cloned.1.call-done = bf16[2048,1408]{1,0:T(8,128)(2,1)} async-done(((bf16[512,1408]{1,0:T(8,128)(2,1)}), bf16[2048,1408]{1,0:T(8,128)(2,1)}) %all-gather.18.cloned.1.call-update) | async-done | bytes 5767184 | tf_op jit(solution)/shard_map/all_gather | solution.py:18
  615.0 106.5 %all-gather.20.cloned.1.call-done = bf16[1408,2048]{1,0:T(8,128)(2,1)} async-done(((bf16[1408,512]{1,0:T(8,128)(2,1)}), bf16[1408,2048]{1,0:T(8,128)(2,1)}) %all-gather.20.cloned.1.call-update) | async-done | bytes 5767184 | tf_op jit(solution)/shard_map/all_gather | solution.py:31
  721.6 7.1 fusion.1
  728.6 0.0 reduce-scatter.5.cloned.1.call-update
  728.6 20.0 %reduce-scatter.5.cloned.1.call-done = bf16[32,2048]{1,0:T(8,128)(2,1)} async-done(((bf16[128,2048]{1,0:T(8,128)(2,1)}), bf16[32,2048]{1,0:T(8,128)(2,1)}) %reduce-scatter.5.cloned.1.call-update) | async-done | bytes 131088 | tf_op jit(solution)/shard_map/reduce_scatter | solution.py:37
  748.7 1.0 add_convert_fusion
  749.7 6.6 all_gather.35
  756.3 0.8 copy.13
  (3 shorter events, 0.0 us)
Async XLA Ops:
  6.5 370.3 %copy-start = (bf16[128,512]{1,0:T(8,128)(2,1)S(1)}, bf16[128,512]{1,0:T(8,128)(2,1)}, u32[]{:S(2)}) copy-start(bf16[128,512]{1,0:T(8,128)(2,1)} %param.12) | copy-start | bytes 393220
  6.5 111.8 %all-gather.8.cloned.1.call-start = ((), (), s32[]{:S(2)}) async-start(), calls=%async_computation.2 | async-start | bytes 7208960 | tf_op jit(solution)/shard_map/all_gather | solution.py:17
  7.3 324.2 %copy-start.1 = (bf16[128,2048]{1,0:T(8,128)(2,1)S(1)}, bf16[128,2048]{1,0:T(8,128)(2,1)}, u32[]{:S(2)}) copy-start(bf16[128,2048]{1,0:T(8,128)(2,1)} %param.11) | copy-start | bytes 1572868
  7.3 324.2 %copy-start.3 = (f32[2048]{0:T(1024)S(1)}, f32[2048]{0:T(1024)}, u32[]{:S(2)}) copy-start(f32[2048]{0:T(1024)} %param.13) | copy-start | bytes 24580
  7.3 217.6 %all-gather.10.cloned.1.call-start = ((), (), s32[]{:S(2)}) async-start(), calls=%async_computation.3 | async-start | bytes 7208960 | tf_op jit(solution)/shard_map/all_gather | solution.py:18
  8.0 323.4 %all-gather.12.cloned.1.call-start = ((), (), s32[]{:S(2)}) async-start(), calls=%async_computation.4 | async-start | bytes 7208960 | tf_op jit(solution)/shard_map/all_gather | solution.py:31
  8.8 368.1 %all-gather.14.cloned.1.call-start = ((), (), s32[]{:S(2)}) async-start(), calls=%async_computation.5 | async-start | bytes 2621440 | tf_op jit(solution)/shard_map/all_gather | solution.py:63
  9.3 391.0 %reduce-scatter.3.cloned.1.call-start = ((), (), s32[]{:S(2)}) async-start(), calls=%async_computation.6 | async-start | bytes 655360 | tf_op jit(solution)/shard_map/reduce_scatter | solution.py:37
  337.8 63.6 %copy-start.4 = (f32[2048]{0:T(1024)S(1)}, f32[2048]{0:T(1024)}, u32[]{:S(2)}) copy-start(f32[2048]{0:T(1024)} %param.18) | copy-start | bytes 24580
  379.7 128.8 %all-gather.16.cloned.1.call-start = ((), (), s32[]{:S(2)}) async-start(), calls=%async_computation.7 | async-start | bytes 7208960 | tf_op jit(solution)/shard_map/all_gather | solution.py:17
  380.3 234.7 %all-gather.18.cloned.1.call-start = ((), (), s32[]{:S(2)}) async-start(), calls=%async_computation.8 | async-start | bytes 7208960 | tf_op jit(solution)/shard_map/all_gather | solution.py:18
  381.0 340.5 %all-gather.20.cloned.1.call-start = ((), (), s32[]{:S(2)}) async-start(), calls=%async_computation.9 | async-start | bytes 7208960 | tf_op jit(solution)/shard_map/all_gather | solution.py:31
  381.8 366.9 %reduce-scatter.5.cloned.1.call-start = ((), (), s32[]{:S(2)}) async-start(), calls=%async_computation.10 | async-start | bytes 655360 | tf_op jit(solution)/shard_map/reduce_scatter | solution.py:37
  512.1 236.6 %copy-start.2 = (bf16[32,2048]{1,0:T(8,128)(2,1)S(1)}, bf16[32,2048]{1,0:T(8,128)(2,1)}, u32[]{:S(2)}) copy-start(bf16[32,2048]{1,0:T(8,128)(2,1)} %reduce-scatter.3.cloned.1.call-done) | copy-start | bytes 393220
Sparse Core Ops, SparseCore 0:
  8.9 109.3 all-gather.7
  119.9 104.9 all-gather.9
  226.5 104.9 all-gather.11
  332.9 43.9 all-gather.13
  379.8 20.4 reduce-scatter.2
  401.7 106.6 all-gather.15
  510.0 104.9 all-gather.17
  616.6 104.9 all-gather.19
  728.8 19.8 reduce-scatter.4
where the time goes:
time: 764 us
  waiting for transfers between devices  708 us (93%)
  matrix products  23.7 us (3%)
  between operations  13.3 us (2%)
  blocking collectives  13.2 us (2%)
    all_gather x2, waiting for transfers between devices, half_branch(): lax.all_gather(down_weight, 'fs', axis=1, tiled=True)  213 us
    all_gather x2, waiting for transfers between devices, gate_values(): lax.all_gather(gate_weight, 'fs', axis=0, tiled=True)  207 us
    all_gather x2, waiting for transfers between devices, gate_values(): lax.all_gather(value_weight, 'fs', axis=0, tiled=True)  206 us
    all_gather x1, waiting for transfers between devices, local(): lax.all_gather(out_weight, 'fs', axis=1, tiled=True)  39.1 us
    reduce_scatter x2, waiting for transfers between devices, share_sum(): lax.psum_scatter(block_terms.astype(jnp.bfloat16), 'tp', scatter_dimensio...  38.5 us
  transfers between devices with their start and end apart: 9, of which 9 were waited for; matrix products, arithmetic and copies ran while one was open for 2% of the time, Pallas kernels for 0%

commit v1 on v0

--- a/solution.py
+++ b/solution.py
@@ -4,6 +4,16 @@
 from jax.sharding import PartitionSpec as P
 
 EPS = 0.1
+
+
+def gather_around(x, axis, dim):
+    ways, here, turn = (lax.axis_size(axis), lax.axis_index(axis), x.shape[dim])
+    lengths = [n * ways if d == dim else n for d, n in enumerate(x.shape)]
+    full = lax.dynamic_update_slice_in_dim(jnp.zeros(lengths, x.dtype), x, here * turn, axis=dim)
+    for far in range(1, ways):
+        x = lax.ppermute(x, axis, [(d, (d + 1) % ways) for d in range(ways)])
+        full = lax.dynamic_update_slice_in_dim(full, x, (here - far) % ways * turn, axis=dim)
+    return full
 
 
 def norm_rows(row_block, gain_vector):
@@ -27,9 +37,7 @@
     gates, values = gate_values(normed, gate_weight, value_weight)
     hidden = (jax.nn.silu(gates) * values).astype(jnp.bfloat16)
     return 0.5 * jnp.dot(
-        hidden,
-        lax.all_gather(down_weight, "fs", axis=1, tiled=True),
-        preferred_element_type=jnp.float32,
+        hidden, gather_around(down_weight, "fs", 1), preferred_element_type=jnp.float32
     )
 
 

time: 764 us -> 687 us (0.90)
  waiting for transfers between devices: 708 us -> 541 us
  starting transfers between devices: 0.31 us -> 65.3 us
  local copies, waits for them, and re-layouts: 0.82 us -> 22.8 us
    ppermute x0 -> x6, waiting for transfers between devices: none -> 314 us  [gather_around(): x = lax.ppermute(x, axis, [(d, (d + 1) % ways) for d in range(ways)])]
    all_gather x2 -> x0, waiting for transfers between devices: 213 us -> none  [half_branch(): lax.all_gather(down_weight, 'fs', axis=1, tiled=True)]
    all_gather x2, waiting for transfers between devices: 207 us -> 15.1 us  [gate_values(): lax.all_gather(gate_weight, 'fs', axis=0, tiled=True)]
    ppermute x0 -> x6, starting transfers between devices: none -> 65.1 us  [gather_around(): x = lax.ppermute(x, axis, [(d, (d + 1) % ways) for d in range(ways)])]
    all_gather x1, waiting for transfers between devices: 39.1 us -> 0.01 us  [local(): lax.all_gather(out_weight, 'fs', axis=1, tiled=True)]
    reduce_scatter x2, waiting for transfers between devices: 38.5 us -> 20 us  [share_sum(): lax.psum_scatter(block_terms.astype(jnp.bfloat16), 'tp', scatter_dimensio...]
    all_gather x2, waiting for transfers between devices: 206 us -> 189 us  [gate_values(): lax.all_gather(value_weight, 'fs', axis=0, tiled=True)]
    dynamic_update_slice x0 -> x8, local copies, waits for them, and re-layouts: none -> 15.5 us  [the longest x6 13.1 us: gather_around(): lax.dynamic_update_slice_in_dim(full, x, (here - far) % ways * turn, axis...]
  transfers between devices with their start and end apart: 9 -> 13, of which waited for: 9 -> 10; matrix products, arithmetic and copies ran while one was open for 2% -> 5% of each run, Pallas kernels for 0% -> 0%
where the time goes in v1:
time: 687 us; the launch traced here: 686 us
  waiting for transfers between devices  541 us (79%)
  starting transfers between devices  65.3 us (10%)
  matrix products  25.6 us (4%)
  local copies, waits for them, and re-layouts  22.8 us (3%)
  blocking collectives  13.8 us (2%)
  between operations  13.6 us (2%)
    ppermute x6, waiting for transfers between devices, gather_around(): x = lax.ppermute(x, axis, [(d, (d + 1) % ways) for d in range(ways)])  314 us
    all_gather x2, waiting for transfers between devices, gate_values(): lax.all_gather(value_weight, 'fs', axis=0, tiled=True)  189 us
    ppermute x6, starting transfers between devices, gather_around(): x = lax.ppermute(x, axis, [(d, (d + 1) % ways) for d in range(ways)])  65.1 us
    reduce_scatter x2, waiting for transfers between devices, share_sum(): lax.psum_scatter(block_terms.astype(jnp.bfloat16), 'tp', scatter_dimensio...  20 us
    all_gather x2, waiting for transfers between devices, gate_values(): lax.all_gather(gate_weight, 'fs', axis=0, tiled=True)  15.1 us
    dot_general x2, matrix products, half_branch(): jnp.dot(hidden, gather_around(down_weight, 'fs', 1), preferred_element_ty...  14.3 us
    all_gather x2, blocking collectives, join_rows(): return lax.all_gather(row_block, 'tp', axis=0, tiled=True)  13.8 us
  transfers between devices with their start and end apart: 13, of which 10 were waited for; matrix products, arithmetic and copies ran while one was open for 5% of the time, Pallas kernels for 0%

profile of v1, /device:TPU:0, one launch (start us, length us, event | category | flops | bytes accessed | tf_op | source)
XLA Modules:
  0.0 686.1 jit_solution(6384695306262801406)
XLA Ops:
  6.5 0.7 all-gather.10.cloned.1.call-update
  7.3 0.0 all-gather.6.cloned.1.call-start
  7.3 0.7 all-gather.6.cloned.1.call-update
  8.0 0.0 all-gather.8.cloned.1.call-start
  8.1 0.7 all-gather.8.cloned.1.call-update
  8.7 0.0 reduce-scatter.3.cloned.1.call-start
  8.8 3.1 collective-permute-start
  11.9 56.6 %collective-permute-done = bf16[1408,512]{1,0:T(8,128)(2,1)} collective-permute-done((bf16[1408,512]{1,0:T(8,128)(2,1)}, bf16[1408,512]{1,0:T(8,128)(2,1)}, u32[]{:S(2)}, u32[]{:S(2)}) %collective-permute-start) | collective-permute-done | bytes 1441824 | tf_op jit(solution)/shard_map/ppermute | solution.py:14
  68.5 9.8 %collective-permute-start.1 = (bf16[1408,512]{1,0:T(8,128)(2,1)}, bf16[1408,512]{1,0:T(8,128)(2,1)S(1)}, u32[]{:S(2)}, u32[]{:S(2)}) collective-permute-start(bf16[1408,512]{1,0:T(8,128)(2,1)} %collective-permute-done), channel_id=1, source_target_pairs={{0,4},{4,8},{8,12},{12,0},{1,5},{5,9},{9,13},{13,1},{2,6},{6,10},{... | collective-permute-start | bytes 4325384 | tf_op jit(solution)/shard_map/ppermute | solution.py:14
  78.3 54.8 %collective-permute-done.1 = bf16[1408,512]{1,0:T(8,128)(2,1)S(1)} collective-permute-done((bf16[1408,512]{1,0:T(8,128)(2,1)}, bf16[1408,512]{1,0:T(8,128)(2,1)S(1)}, u32[]{:S(2)}, u32[]{:S(2)}) %collective-permute-start.1) | collective-permute-done | bytes 1441824 | tf_op jit(solution)/shard_map/ppermute | solution.py:14
  133.1 24.5 %collective-permute-start.2 = (bf16[1408,512]{1,0:T(8,128)(2,1)S(1)}, bf16[1408,512]{1,0:T(8,128)(2,1)}, u32[]{:S(2)}, u32[]{:S(2)}) collective-permute-start(bf16[1408,512]{1,0:T(8,128)(2,1)S(1)} %collective-permute-done.1), channel_id=1, source_target_pairs={{0,4},{4,8},{8,12},{12,0},{1,5},{5,9},{9,13},{13,1},{2,6},{6,10},{... | collective-permute-start | bytes 4325384 | tf_op jit(solution)/shard_map/ppermute | solution.py:14
  157.6 1.2 fusion.5
  158.9 3.2 broadcast.36.clone.1
  162.1 1.2 constant_dynamic-update-slice_fusion.7
  163.3 2.7 constant_dynamic-update-slice_fusion.6
  166.0 1.2 constant_dynamic-update-slice_fusion.5
  167.2 3.0 fusion.16
  170.3 48.3 %collective-permute-done.2 = bf16[1408,512]{1,0:T(8,128)(2,1)} collective-permute-done((bf16[1408,512]{1,0:T(8,128)(2,1)S(1)}, bf16[1408,512]{1,0:T(8,128)(2,1)}, u32[]{:S(2)}, u32[]{:S(2)}) %collective-permute-start.2) | collective-permute-done | bytes 1441824 | tf_op jit(solution)/shard_map/ppermute | solution.py:14
  218.5 2.7 constant_dynamic-update-slice_fusion.4
  221.2 15.1 %all-gather.6.cloned.1.call-done = bf16[2048,1408]{1,0:T(8,128)(2,1)} async-done(((bf16[512,1408]{1,0:T(8,128)(2,1)}), bf16[2048,1408]{1,0:T(8,128)(2,1)}) %all-gather.6.cloned.1.call-update) | async-done | bytes 5767184 | tf_op jit(solution)/shard_map/all_gather | solution.py:27
  236.3 4.5 fusion.12
  240.9 102.0 %all-gather.8.cloned.1.call-done = bf16[2048,1408]{1,0:T(8,128)(2,1)} async-done(((bf16[512,1408]{1,0:T(8,128)(2,1)}), bf16[2048,1408]{1,0:T(8,128)(2,1)}) %all-gather.8.cloned.1.call-update) | async-done | bytes 5767184 | tf_op jit(solution)/shard_map/all_gather | solution.py:28
  342.9 7.3 %fusion.1 = bf16[128,2048]{1,0:T(8,128)(2,1)} fusion(f32[128,2048]{1,0:T(8,128)S(1)} %copy-done.5, bf16[1408,2048]{1,0:T(8,128)(2,1)} %constant_dynamic-update-slice_fusion.4, bf16[2048,1408]{1,0:T(8,128)(2,1)} %all-gather.8.cloned.1.call-done, f32[128,1408]{1,0:T(8,128)} %fusion.12, bf16[128,2048]{1,0:T(8,128)(2,1)S(1)} %copy-done.1, ...), kind=kOutput, calls=%fused_computation.5 | convolution fusion | flops 1479311360 | bytes 14361088 | tf_op jit(solution)/shard_map/dot_general | solution.py:39
  350.2 0.0 all-gather.12.cloned.1.call-start
  350.2 0.5 all-gather.12.cloned.1.call-update
  350.8 0.0 all-gather.14.cloned.1.call-start
  350.8 0.5 all-gather.14.cloned.1.call-update
  351.4 0.0 reduce-scatter.5.cloned.1.call-start
  351.4 0.1 collective-permute-start.3
  351.5 38.1 %collective-permute-done.3 = bf16[1408,512]{1,0:T(8,128)(2,1)S(1)} collective-permute-done((bf16[1408,512]{1,0:T(8,128)(2,1)S(1)}, bf16[1408,512]{1,0:T(8,128)(2,1)S(1)}, u32[]{:S(2)}, u32[]{:S(2)}) %collective-permute-start.3) | collective-permute-done | bytes 1441824 | tf_op jit(solution)/shard_map/ppermute | solution.py:14
  389.6 65.9 %collective-permute-done.4 = bf16[1408,512]{1,0:T(8,128)(2,1)} collective-permute-done((bf16[1408,512]{1,0:T(8,128)(2,1)S(1)}, bf16[1408,512]{1,0:T(8,128)(2,1)}, u32[]{:S(2)}, u32[]{:S(2)}) %collective-permute-start.4) | collective-permute-done | bytes 1441824 | tf_op jit(solution)/shard_map/ppermute | solution.py:14
  455.5 27.6 %collective-permute-start.5 = (bf16[1408,512]{1,0:T(8,128)(2,1)}, bf16[1408,512]{1,0:T(8,128)(2,1)}, u32[]{:S(2)}, u32[]{:S(2)}) collective-permute-start(bf16[1408,512]{1,0:T(8,128)(2,1)} %collective-permute-done.4), channel_id=1, source_target_pairs={{0,4},{4,8},{8,12},{12,0},{1,5},{5,9},{9,13},{13,1},{2,6},{6,10},{... | collective-permute-start | bytes 4325384 | tf_op jit(solution)/shard_map/ppermute | solution.py:14
  483.1 3.2 broadcast.36.clone
  486.3 1.2 constant_dynamic-update-slice_fusion.3
  487.6 1.3 constant_dynamic-update-slice_fusion.2
  488.9 2.6 constant_dynamic-update-slice_fusion.1
  491.4 50.1 %collective-permute-done.5 = bf16[1408,512]{1,0:T(8,128)(2,1)} collective-permute-done((bf16[1408,512]{1,0:T(8,128)(2,1)}, bf16[1408,512]{1,0:T(8,128)(2,1)}, u32[]{:S(2)}, u32[]{:S(2)}) %collective-permute-start.5) | collective-permute-done | bytes 1441824 | tf_op jit(solution)/shard_map/ppermute | solution.py:14
  541.5 2.6 constant_dynamic-update-slice_fusion
  544.2 1.1 multiply_reduce_fusion
  545.3 1.0 multiply_convert_fusion
  546.3 7.1 %all_gather.24 = bf16[128,2048]{1,0:T(8,128)(2,1)S(1)} all-gather(bf16[32,2048]{1,0:T(8,128)(2,1)S(1)} %multiply_convert_fusion), channel_id=1, replica_groups=mesh['grp'=2,'fs'=4,'tp'=4] {'tp'}, dimensions={0}, use_global_device_ids=true | all-gather | bytes 655360 | tf_op jit(solution)/shard_map/all_gather | solution.py:51
  553.4 3.7 fusion.17
  557.1 86.7 %all-gather.14.cloned.1.call-done = bf16[2048,1408]{1,0:T(8,128)(2,1)} async-done(((bf16[512,1408]{1,0:T(8,128)(2,1)}), bf16[2048,1408]{1,0:T(8,128)(2,1)}) %all-gather.14.cloned.1.call-update) | async-done | bytes 5767184 | tf_op jit(solution)/shard_map/all_gather | solution.py:28
  643.8 7.1 %fusion.2 = bf16[128,2048]{1,0:T(8,128)(2,1)} fusion(bf16[1408,2048]{1,0:T(8,128)(2,1)} %constant_dynamic-update-slice_fusion, bf16[128,2048]{1,0:T(8,128)(2,1)S(1)} %all_gather.24, bf16[2048,1408]{1,0:T(8,128)(2,1)} %all-gather.14.cloned.1.call-done, f32[128,1408]{1,0:T(8,128)S(1)} %fusion.17), kind=kOutput, calls=%fused_computation.6 | convolution fusion | flops 1478000640 | bytes 13303808 | tf_op jit(solution)/shard_map/dot_general | solution.py:39
  650.9 20.0 %reduce-scatter.5.cloned.1.call-done = bf16[32,2048]{1,0:T(8,128)(2,1)} async-done(((bf16[128,2048]{1,0:T(8,128)(2,1)}), bf16[32,2048]{1,0:T(8,128)(2,1)}) %reduce-scatter.5.cloned.1.call-update) | async-done | bytes 131088 | tf_op jit(solution)/shard_map/reduce_scatter | solution.py:45
  670.9 1.0 add_convert_fusion
  671.9 6.6 all_gather.27
  678.5 0.8 copy.21
  (25 shorter events, 0.1 us)
Async XLA Ops:
  6.5 160.7 %copy-start = (bf16[128,512]{1,0:T(8,128)(2,1)S(1)}, bf16[128,512]{1,0:T(8,128)(2,1)}, u32[]{:S(2)}) copy-start(bf16[128,512]{1,0:T(8,128)(2,1)} %param.12) | copy-start | bytes 393220
  6.5 155.5 %copy-start.2 = (bf16[1408,512]{1,0:T(8,128)(2,1)S(1)}, bf16[1408,512]{1,0:T(8,128)(2,1)}, u32[]{:S(2)}) copy-start(bf16[1408,512]{1,0:T(8,128)(2,1)} %param.16) | copy-start | bytes 4325380
  6.5 160.7 %all-gather.10.cloned.1.call-start = ((), (), s32[]{:S(2)}) async-start(), calls=%async_computation.4 | async-start | bytes 2621440 | tf_op jit(solution)/shard_map/all_gather | solution.py:71
  7.3 229.1 %all-gather.6.cloned.1.call-start = ((), (), s32[]{:S(2)}) async-start(), calls=%async_computation.2 | async-start | bytes 7208960 | tf_op jit(solution)/shard_map/all_gather | solution.py:27
  8.0 334.9 %all-gather.8.cloned.1.call-start = ((), (), s32[]{:S(2)}) async-start(), calls=%async_computation.3 | async-start | bytes 7208960 | tf_op jit(solution)/shard_map/all_gather | solution.py:28
  8.7 535.4 %reduce-scatter.3.cloned.1.call-start = ((), (), s32[]{:S(2)}) async-start(), calls=%async_computation.5 | async-start | bytes 655360 | tf_op jit(solution)/shard_map/reduce_scatter | solution.py:45
  8.8 59.8 %collective-permute-start = (bf16[1408,512]{1,0:T(8,128)(2,1)}, bf16[1408,512]{1,0:T(8,128)(2,1)}, u32[]{:S(2)}, u32[]{:S(2)}) collective-permute-start(bf16[1408,512]{1,0:T(8,128)(2,1)} %param.16), channel_id=1, source_target_pairs={{0,4},{4,8},{8,12},{12,0},{1,5},{5,9},{9,13},{13,1},{2,6},{6,10},{... | collective-permute-start | bytes 4325384 | tf_op jit(solution)/shard_map/ppermute | solution.py:14
  68.5 64.6 %collective-permute-start.1 = (bf16[1408,512]{1,0:T(8,128)(2,1)}, bf16[1408,512]{1,0:T(8,128)(2,1)S(1)}, u32[]{:S(2)}, u32[]{:S(2)}) collective-permute-start(bf16[1408,512]{1,0:T(8,128)(2,1)} %collective-permute-done), channel_id=1, source_target_pairs={{0,4},{4,8},{8,12},{12,0},{1,5},{5,9},{9,13},{13,1},{2,6},{6,10},{... | collective-permute-start | bytes 4325384 | tf_op jit(solution)/shard_map/ppermute | solution.py:14
  133.1 85.4 %collective-permute-start.2 = (bf16[1408,512]{1,0:T(8,128)(2,1)S(1)}, bf16[1408,512]{1,0:T(8,128)(2,1)}, u32[]{:S(2)}, u32[]{:S(2)}) collective-permute-start(bf16[1408,512]{1,0:T(8,128)(2,1)S(1)} %collective-permute-done.1), channel_id=1, source_target_pairs={{0,4},{4,8},{8,12},{12,0},{1,5},{5,9},{9,13},{13,1},{2,6},{6,10},{... | collective-permute-start | bytes 4325384 | tf_op jit(solution)/shard_map/ppermute | solution.py:14
  163.3 73.0 %copy-start.1 = (bf16[128,2048]{1,0:T(8,128)(2,1)S(1)}, bf16[128,2048]{1,0:T(8,128)(2,1)}, u32[]{:S(2)}) copy-start(bf16[128,2048]{1,0:T(8,128)(2,1)} %param.11) | copy-start | bytes 1572868
  163.3 73.0 %copy-start.6 = (f32[2048]{0:T(1024)S(1)}, f32[2048]{0:T(1024)}, u32[]{:S(2)}) copy-start(f32[2048]{0:T(1024)} %param.13) | copy-start | bytes 24580
  218.5 124.4 %copy-start.5 = (f32[128,2048]{1,0:T(8,128)S(1)}, f32[128,2048]{1,0:T(8,128)}, u32[]{:S(2)}) copy-start(f32[128,2048]{1,0:T(8,128)} %fusion.16) | copy-start | bytes 3145732
  240.9 110.6 %copy-start.3 = (bf16[1408,512]{1,0:T(8,128)(2,1)S(1)}, bf16[1408,512]{1,0:T(8,128)(2,1)}, u32[]{:S(2)}) copy-start(bf16[1408,512]{1,0:T(8,128)(2,1)} %param.21) | copy-start | bytes 4325380
  350.2 203.2 %all-gather.12.cloned.1.call-start = ((), (), s32[]{:S(2)}) async-start(), calls=%async_computation.6 | async-start | bytes 7208960 | tf_op jit(solution)/shard_map/all_gather | solution.py:27
  350.8 293.0 %all-gather.14.cloned.1.call-start = ((), (), s32[]{:S(2)}) async-start(), calls=%async_computation.7 | async-start | bytes 7208960 | tf_op jit(solution)/shard_map/all_gather | solution.py:28
  351.4 319.6 %reduce-scatter.5.cloned.1.call-start = ((), (), s32[]{:S(2)}) async-start(), calls=%async_computation.8 | async-start | bytes 655360 | tf_op jit(solution)/shard_map/reduce_scatter | solution.py:45
  351.4 38.1 %collective-permute-start.3 = (bf16[1408,512]{1,0:T(8,128)(2,1)S(1)}, bf16[1408,512]{1,0:T(8,128)(2,1)S(1)}, u32[]{:S(2)}, u32[]{:S(2)}) collective-permute-start(bf16[1408,512]{1,0:T(8,128)(2,1)S(1)} %copy-done.3), channel_id=1, source_target_pairs={{0,4},{4,8},{8,12},{12,0},{1,5},{5,9},{9,13},{13,1},{2,6},{6,10},{... | collective-permute-start | bytes 4325384 | tf_op jit(solution)/shard_map/ppermute | solution.py:14
  389.6 65.9 %collective-permute-start.4 = (bf16[1408,512]{1,0:T(8,128)(2,1)S(1)}, bf16[1408,512]{1,0:T(8,128)(2,1)}, u32[]{:S(2)}, u32[]{:S(2)}) collective-permute-start(bf16[1408,512]{1,0:T(8,128)(2,1)S(1)} %collective-permute-done.3), channel_id=1, source_target_pairs={{0,4},{4,8},{8,12},{12,0},{1,5},{5,9},{9,13},{13,1},{2,6},{6,10},{... | collective-permute-start | bytes 4325384 | tf_op jit(solution)/shard_map/ppermute | solution.py:14
  455.5 86.0 %collective-permute-start.5 = (bf16[1408,512]{1,0:T(8,128)(2,1)}, bf16[1408,512]{1,0:T(8,128)(2,1)}, u32[]{:S(2)}, u32[]{:S(2)}) collective-permute-start(bf16[1408,512]{1,0:T(8,128)(2,1)} %collective-permute-done.4), channel_id=1, source_target_pairs={{0,4},{4,8},{8,12},{12,0},{1,5},{5,9},{9,13},{13,1},{2,6},{6,10},{... | collective-permute-start | bytes 4325384 | tf_op jit(solution)/shard_map/ppermute | solution.py:14
  486.3 58.9 %copy-start.7 = (f32[2048]{0:T(1024)S(1)}, f32[2048]{0:T(1024)}, u32[]{:S(2)}) copy-start(f32[2048]{0:T(1024)} %param.18) | copy-start | bytes 24580
  557.1 113.8 %copy-start.4 = (bf16[32,2048]{1,0:T(8,128)(2,1)S(1)}, bf16[32,2048]{1,0:T(8,128)(2,1)}, u32[]{:S(2)}) copy-start(bf16[32,2048]{1,0:T(8,128)(2,1)} %reduce-scatter.3.cloned.1.call-done) | copy-start | bytes 393220
Sparse Core Ops, SparseCore 0:
  8.9 70.9 all-gather.9
  81.5 154.7 all-gather.5
  237.9 104.9 all-gather.7
  350.3 19.8 reduce-scatter.2
  371.7 165.0 all-gather.11
  538.2 105.5 all-gather.13
  651.0 19.8 reduce-scatter.4
